TPU v7x, 32 devices: a whole 2x2x4 slice. The times are simulated.
32 devices in a mesh: ep: 4 (over y, x), tp: 8 (over z, core).
Axes of the slice: x: 2, y: 2, z: 4, core: 2. Of those that a mesh axis runs over, the one named last changes fastest.
Arguments:
- tokens: bfloat16 [64, 4096], P('ep'), may hold values from -6 to 6
- attn_gain: float32 [4096], replicated, may hold values from 0.1 to 1.9
- w_query: bfloat16 [4096, 2048], P('ep', 'tp'), may hold values from -0.15625 to 0.15625
- w_key: bfloat16 [4096, 2048], P('ep', 'tp'), may hold values from -0.09375 to 0.09375
- w_value: bfloat16 [4096, 2048], P('ep', 'tp'), may hold values from -0.09375 to 0.09375
- mix_lambda: float32 [16], P('tp'), may hold values from 0.3 to 0.8
- head_gain: float32 [128], replicated, may hold values from 0.1 to 1.9
- w_output: bfloat16 [2048, 4096], P('tp'), may hold values from -0.125 to 0.125
- cache_keys: bfloat16 [64, 1024, 2048], P('ep', None, 'tp'), may hold values from -180 to 180
- cache_value: bfloat16 [64, 1024, 2048], P('ep', None, 'tp'), may hold values from -6 to 6
- lengths: int32 [64], P('ep'), may hold values from 1 to 1024
- moe_gain: float32 [4096], replicated, may hold values from 0.1 to 1.9
- group_ids: int32 [64], P('ep'), may hold values from 0 to 1, as said below
- member_ids: int32 [64, 2], P('ep'), may hold values from 0 to 1, as said below
- group_gate: float32 [64], P('ep'), may hold values from 0.3 to 1
- member_logits: float32 [64, 2], P('ep'), may hold values from -4 to 4
- w_exp_gate: bfloat16 [4, 4096, 2048], P('ep', None, 'tp'), may hold values from -0.09375 to 0.09375
- w_exp_up: bfloat16 [4, 4096, 2048], P('ep', None, 'tp'), may hold values from -0.09375 to 0.09375
- w_exp_down: bfloat16 [4, 2048, 4096], P('ep', 'tp'), may hold values from -0.125 to 0.125
Outputs:
- mixed: bfloat16 [64, 4096], P('ep', 'tp')
- fresh_keys: bfloat16 [64, 2048], P('ep', 'tp')
- fresh_value: bfloat16 [64, 2048], P('ep', 'tp')
Inputs may be any that keep to these rules, and one draw needn't show every extreme that they name: `group_ids`: each index of ep holds 16 consecutive tokens, of which every group gets the same number. A token's 2 members differ, and every expert group_ids * 2 + member_ids receives exactly 8 of the token-expert pairs of each index of ep.
All inputs are finite; a program needn't handle non-finite values.
Results may differ from a plain program's by a relative error of at most 0.015.
The roundings to bfloat16 on the way count: a program that leaves them out, or rounds other values in their place, can miss the bound.
Values may be sent and summed in bfloat16 or wider, within the bound.
A program may use at most 64 MiB of HBM per device.

v0:
```python
import jax
import jax.numpy as jnp
from jax import lax
from jax.sharding import PartitionSpec as P

EPG = 2
EPS = 1e-06


def rms_scale(values, gain):
    return values * lax.rsqrt(jnp.mean(values * values, axis=-1, keepdims=True) + EPS) * gain


def on_device(
    tokens,
    attn_gain,
    w_query,
    w_key,
    w_value,
    mix_lambda,
    head_gain,
    w_output,
    cache_keys,
    cache_value,
    lengths,
    moe_gain,
    group_ids,
    member_ids,
    group_gate,
    member_logits,
    w_exp_gate,
    w_exp_up,
    w_exp_down,
):
    seqs, width = tokens.shape
    resid_in = tokens.astype(jnp.float32)
    normed = rms_scale(resid_in, attn_gain).astype(jnp.bfloat16)
    heads_local = mix_lambda.shape[0]
    qk_cols = w_query.shape[1]
    head_dim = qk_cols // (2 * heads_local)
    stacked = jnp.concatenate([w_query, w_key, w_value], axis=1)
    sliced = lax.all_to_all(normed, "ep", split_axis=1, concat_axis=0, tiled=True)
    projected = lax.psum_scatter(
        jnp.dot(sliced, stacked, preferred_element_type=jnp.float32),
        "ep",
        scatter_dimension=0,
        tiled=True,
    )
    projected = projected.astype(jnp.bfloat16)
    query = projected[:, :qk_cols]
    fresh_keys = projected[:, qk_cols : 2 * qk_cols]
    fresh_value = projected[:, 2 * qk_cols :]
    positions_all = cache_keys.shape[1]
    total_heads = heads_local * lax.axis_size("tp")
    head_index = (lax.axis_index("tp") * heads_local + jnp.arange(heads_local)).astype(jnp.float32)
    slopes = 2.0 ** (-8.0 * (head_index + 1.0) / total_heads)
    scale = head_dim ** (-0.5)
    positions = jnp.arange(positions_all)
    dist = (lengths[:, None] - positions[None, :]).astype(jnp.float32)
    valid = positions[None, :] < lengths[:, None]
    query4 = query.reshape(seqs, heads_local, 2, head_dim)
    keys5 = cache_keys.reshape(seqs, positions_all, heads_local, 2, head_dim)
    old = jnp.einsum("shcd,slhcd->cshl", query4, keys5, preferred_element_type=jnp.float32) * scale
    old = old - slopes[None, None, :, None] * dist[None, :, None, :]
    old = jnp.where(valid[None, :, None, :], old, -jnp.inf)
    fresh4 = fresh_keys.reshape(seqs, heads_local, 2, head_dim).astype(jnp.float32)
    new = jnp.moveaxis(jnp.sum(query4.astype(jnp.float32) * fresh4, axis=-1) * scale, 2, 0)
    full = jnp.concatenate([old, new[..., None]], axis=-1)
    maps = jax.nn.softmax(full, axis=-1)
    weights = (maps[0] - mix_lambda[None, :, None] * maps[1]).astype(jnp.bfloat16)
    values = cache_value.reshape(seqs, positions_all, heads_local, 2 * head_dim)
    head_mix = jnp.einsum(
        "shl,slhe->she", weights[..., :positions_all], values, preferred_element_type=jnp.float32
    )
    head_mix = head_mix + weights[..., positions_all].astype(jnp.float32)[
        ..., None
    ] * fresh_value.reshape(seqs, heads_local, 2 * head_dim).astype(jnp.float32)
    head_out = (
        rms_scale(head_mix, head_gain)
        .astype(jnp.bfloat16)
        .reshape(seqs, heads_local * 2 * head_dim)
    )
    term = jnp.dot(head_out, w_output, preferred_element_type=jnp.float32).astype(jnp.bfloat16)
    attn_sum = lax.psum(
        lax.optimization_barrier(term).astype(jnp.float32).astype(jnp.bfloat16), "tp"
    ).astype(jnp.float32)
    resid = resid_in + attn_sum
    moe_in = rms_scale(resid, moe_gain).astype(jnp.bfloat16)
    top = member_ids.shape[1]
    experts_local = w_exp_gate.shape[0]
    ep_count = lax.axis_size("ep")
    experts_all = experts_local * ep_count
    capacity = seqs * top // experts_all
    expert_ids = group_ids[:, None] * EPG + member_ids
    route_weight = jax.nn.softmax(member_logits, axis=-1) * group_gate[:, None]
    flat_ids = expert_ids.reshape(seqs * top)
    onehot = (flat_ids[:, None] == jnp.arange(experts_all)[None, :]).astype(jnp.int32)
    ranks = jnp.sum(jnp.cumsum(onehot, axis=0) * onehot, axis=1) - 1
    slot_grid = (flat_ids * capacity + ranks).reshape(seqs, top)
    slot_range = jnp.arange(experts_all * capacity)
    picker = jnp.sum((slot_grid[None, :, :] == slot_range[:, None, None]).astype(jnp.int32), axis=2)
    dispatch = jnp.dot(
        picker.astype(jnp.bfloat16), moe_in, preferred_element_type=jnp.float32
    ).astype(jnp.bfloat16)
    dispatch = dispatch.reshape(ep_count, experts_local, capacity, width)
    received = lax.all_to_all(dispatch, "ep", split_axis=0, concat_axis=2, tiled=True)
    received = received.reshape(experts_local, ep_count * capacity, width)
    gate = jnp.einsum("erd,edf->erf", received, w_exp_gate, preferred_element_type=jnp.float32)
    upper = jnp.einsum("erd,edf->erf", received, w_exp_up, preferred_element_type=jnp.float32)
    hidden = (jax.nn.silu(gate) * upper).astype(jnp.bfloat16)
    down = jnp.einsum("erf,efd->erd", hidden, w_exp_down, preferred_element_type=jnp.float32)
    summed = lax.psum_scatter(down.astype(jnp.bfloat16), "tp", scatter_dimension=2, tiled=True)
    cols = summed.shape[2]
    returned = lax.all_to_all(
        summed.reshape(experts_local, ep_count, capacity, cols),
        "ep",
        split_axis=1,
        concat_axis=0,
        tiled=True,
    )
    returned = returned.reshape(experts_all * capacity, cols)
    picked = returned[slot_grid].astype(jnp.float32)
    routed = jnp.sum(picked * route_weight[:, :, None], axis=1)
    own = lax.dynamic_slice_in_dim(resid, lax.axis_index("tp") * cols, cols, 1)
    mixed = (own + routed).astype(jnp.bfloat16)
    return (mixed, fresh_keys, fresh_value)


def solution(mesh):
    return jax.shard_map(
        on_device,
        mesh=mesh,
        in_specs=(
            P("ep", None),
            P(),
            P("ep", "tp"),
            P("ep", "tp"),
            P("ep", "tp"),
            P("tp"),
            P(),
            P("tp", None),
            P("ep", None, "tp"),
            P("ep", None, "tp"),
            P("ep"),
            P(),
            P("ep"),
            P("ep", None),
            P("ep"),
            P("ep", None),
            P("ep", None, "tp"),
            P("ep", None, "tp"),
            P("ep", "tp", None),
        ),
        out_specs=(P("ep", "tp"), P("ep", "tp"), P("ep", "tp")),
        check_vma=False,
    )
```

profile of v0, /device:TPU:0, one launch (start us, length us, event | category | flops | bytes accessed | tf_op | source)
XLA Modules:
  0.0 177.5 jit_solution(10258000634573673739)
XLA Ops:
  7.2 1.2 fusion.27
  8.4 1.0 fusion.29
  9.4 0.6 copy.110
  10.0 5.2 %all-to-all-start = ((bf16[16,4,1024]{2,0,1:T(8,128)(2,1)}), bf16[16,4,1024]{2,0,1:T(8,128)(2,1)S(1)}, u32[]{:S(2)}, u32[]{:S(2)}) async-start(bf16[16,4,1024]{2,0,1:T(8,128)(2,1)} %bitcast.80), calls=%async_computation | async-start | bytes 262144 | tf_op jit(solution)/shard_map/all_to_all | solution.py:42
  15.2 0.7 subtract_convert_fusion
  16.0 0.8 copy.78
  16.7 0.7 broadcast_multiply_fusion.1
  17.7 0.2 select_reduce_fusion
  18.0 2.2 %all-to-all-done = bf16[16,4,1024]{2,0,1:T(8,128)(2,1)S(1)} async-done(((bf16[16,4,1024]{2,0,1:T(8,128)(2,1)}), bf16[16,4,1024]{2,0,1:T(8,128)(2,1)S(1)}, u32[]{:S(2)}, u32[]{:S(2)}) %all-to-all-start) | async-done | bytes 131104 | tf_op jit(solution)/shard_map/all_to_all | solution.py:42
  20.3 2.5 %fusion.12 = f32[64,768]{1,0:T(8,128)} fusion(bf16[64,1024]{1,0:T(8,128)(2,1)S(1)} %bitcast.84, bf16[1024,256]{1,0:T(8,128)(2,1)} %param.23, bf16[1024,256]{1,0:T(8,128)(2,1)} %param.22, bf16[1024,256]{1,0:T(8,128)(2,1)} %param.21), kind=kOutput, calls=%fused_computation.16 | convolution fusion | flops 105381888 | bytes 1900544 | tf_op jit(solution)/shard_map/dot_general | solution.py:44
  22.9 12.3 %copy.74 = bf16[16,1024,256]{1,2,0:T(8,128)(2,1)} copy(bf16[16,1024,256]{2,1,0:T(8,128)(2,1)} %param.27) | data formatting | bytes 16777216 | tf_op args[8]
  35.4 11.5 %reduce-scatter.3.cloned.1.call-done = f32[16,768]{1,0:T(8,128)} async-done(((f32[64,768]{1,0:T(8,128)}), f32[16,768]{1,0:T(8,128)}) %reduce-scatter.3.cloned.1.call-update) | async-done | bytes 49168 | tf_op jit(solution)/shard_map/reduce_scatter | solution.py:43
  46.9 0.8 convert_element_type.87
  48.2 4.6 %fusion.3 = f32[2,16,2,1,1024]{4,3,2,1,0:T(1,128)S(1)} fusion(bf16[16,1024,2,2,64]{1,4,3,2,0:T(8,128)(2,1)} %bitcast.81, bf16[16,2,2,64,1]{3,2,1,0,4:T(2,128)(2,1)S(1)} %reshape.201), kind=kOutput, calls=%fused_computation.4 | convolution fusion | flops 8388608 | bytes 8658944 | tf_op jit(solution)/shard_map/shcd,slhcd->cshl/dot_general | solution.py:63
  52.8 0.2 fusion.66
  53.1 0.8 fusion.35
  54.1 0.2 copy.89
  54.3 4.7 %fusion = f32[16,2,1,128]{3,2,1,0:T(1,128)S(1)} fusion(bf16[16,2,1024,1]{2,0,1,3:T(8,128)(2,1)S(1)} %slice_bitcast_fusion.2, bf16[16,1024,256]{2,1,0:T(8,128)(2,1)} %param.28), kind=kOutput, calls=%fused_computation.1 | convolution fusion | flops 8388608 | bytes 8470528 | tf_op jit(solution)/shard_map/shl,slhe->she/dot_general | solution.py:72
  59.0 0.2 multiply_reduce_fusion.3
  59.3 1.0 convolution_convert_fusion.2
  60.5 55.0 %all-reduce.2.cloned.1.call-done = bf16[16,4096]{1,0:T(8,128)(2,1)} async-done(((bf16[16,4096]{1,0:T(8,128)(2,1)}), bf16[16,4096]{1,0:T(8,128)(2,1)}) %all-reduce.2.cloned.1.call-update) | async-done | bytes 131088 | tf_op jit(solution)/shard_map/psum | solution.py:84
  115.5 1.1 convert_add_fusion
  116.6 1.2 fusion.5
  117.8 9.2 %all_to_all.37 = bf16[4,1,8,4096]{3,2,1,0:T(8,128)(2,1)S(1)} all-to-all(bf16[4,1,8,4096]{3,2,1,0:T(8,128)(2,1)S(1)} %fusion.5), channel_id=1, replica_groups=mesh['ep'=4,'tp'=8] {'ep'}, dimensions={0} | all-to-all | bytes 524288 | tf_op jit(solution)/shard_map/all_to_all | solution.py:106
  126.9 2.0 %fusion.10 = f32[32,256]{1,0:T(8,128)S(1)} fusion(bf16[1,4096,256]{2,1,0:T(8,128)(2,1)} %param.35, bf16[4,1,8,4096]{3,2,1,0:T(8,128)(2,1)S(1)} %all_to_all.37), kind=kOutput, calls=%fused_computation.14 | convolution fusion | flops 67108864 | bytes 2392064 | tf_op jit(solution)/shard_map/erd,edf->erf/dot_general | solution.py:108
  129.0 3.6 %fusion.6 = bf16[1,32,4096]{2,1,0:T(8,128)(2,1)} fusion(bf16[1,256,4096]{2,1,0:T(8,128)(2,1)S(1)} %copy-done, bf16[1,4096,256]{2,1,0:T(8,128)(2,1)} %param.36, bf16[4,1,8,4096]{3,2,1,0:T(8,128)(2,1)S(1)} %all_to_all.37, f32[32,256]{1,0:T(8,128)S(1)} %fusion.10), kind=kOutput, calls=%fused_computation.9 | convolution fusion | flops 134397952 | bytes 4751360 | tf_op jit(solution)/shard_map/erf,efd->erd/dot_general | solution.py:111
  132.8 28.4 %reduce-scatter.5.cloned.1.call-done = bf16[1,32,512]{2,1,0:T(8,128)(2,1)} async-done(((bf16[1,32,4096]{2,1,0:T(8,128)(2,1)}), bf16[1,32,512]{2,1,0:T(8,128)(2,1)}) %reduce-scatter.5.cloned.1.call-update) | async-done | bytes 32784 | tf_op jit(solution)/shard_map/reduce_scatter | solution.py:112
  161.1 3.7 %all-to-all-start.2 = ((bf16[1,4,8,512]{3,2,0,1:T(8,128)(2,1)}), bf16[1,4,8,512]{3,2,0,1:T(8,128)(2,1)S(1)}, u32[]{:S(2)}, u32[]{:S(2)}) async-start(bf16[1,4,8,512]{3,2,0,1:T(8,128)(2,1)} %bitcast.90), calls=%async_computation.4 | async-start | bytes 65536 | tf_op jit(solution)/shard_map/all_to_all | solution.py:114
  164.9 4.7 %all-to-all-done.2 = bf16[1,4,8,512]{3,2,0,1:T(8,128)(2,1)S(1)} async-done(((bf16[1,4,8,512]{3,2,0,1:T(8,128)(2,1)}), bf16[1,4,8,512]{3,2,0,1:T(8,128)(2,1)S(1)}, u32[]{:S(2)}, u32[]{:S(2)}) %all-to-all-start.2) | async-done | bytes 32800 | tf_op jit(solution)/shard_map/all_to_all | solution.py:114
  169.5 0.6 gather_fusion
  170.2 0.1 multiply_reduce_fusion.1
  170.4 0.6 add_convert_fusion
  (64 shorter events, 2.1 us)
Async XLA Ops:
  7.2 121.8 %copy-start = (bf16[1,256,4096]{2,1,0:T(8,128)(2,1)S(1)}, bf16[1,256,4096]{2,1,0:T(8,128)(2,1)}, u32[]{:S(2)}) copy-start(bf16[1,256,4096]{2,1,0:T(8,128)(2,1)} %param.37) | copy-start | bytes 6291460
  10.0 10.2 %all-to-all-start = ((bf16[16,4,1024]{2,0,1:T(8,128)(2,1)}), bf16[16,4,1024]{2,0,1:T(8,128)(2,1)S(1)}, u32[]{:S(2)}, u32[]{:S(2)}) async-start(bf16[16,4,1024]{2,0,1:T(8,128)(2,1)} %bitcast.80), calls=%async_computation | async-start | bytes 262144 | tf_op jit(solution)/shard_map/all_to_all | solution.py:42
  15.2 31.7 %reduce-scatter.3.cloned.1.call-start = ((), (), s32[]{:S(2)}) async-start(), calls=%async_computation.5 | async-start | bytes 245760 | tf_op jit(solution)/shard_map/reduce_scatter | solution.py:43
  20.3 2.6 %copy-start.7 = (s32[16]{0:T(128)S(1)}, s32[16]{0:T(128)}, u32[]{:S(2)}) copy-start(s32[16]{0:T(128)} %param.29) | copy-start | bytes 196
  22.8 92.7 %all-reduce.2.cloned.1.call-start = ((), (), s32[]{:S(2)}) async-start(), calls=%async_computation.6 | async-start | bytes 262144 | tf_op jit(solution)/shard_map/psum | solution.py:84
  47.7 5.1 %copy-start.4 = (bf16[16,256]{1,0:T(8,128)(2,1)}, bf16[16,256]{1,0:T(8,128)(2,1)S(1)}, u32[]{:S(2)}) copy-start(bf16[16,256]{1,0:T(8,128)(2,1)S(1)} %get-tuple-element.10) | copy-start | bytes 24580
  47.7 6.5 %copy-start.3 = (bf16[16,256]{1,0:T(8,128)(2,1)}, bf16[16,256]{1,0:T(8,128)(2,1)S(1)}, u32[]{:S(2)}) copy-start(bf16[16,256]{1,0:T(8,128)(2,1)S(1)} %get-tuple-element.9) | copy-start | bytes 24580
  52.8 1.1 copy-start.8
  54.3 4.9 %copy-start.9 = (f32[128]{0:T(128)S(1)}, f32[128]{0:T(128)}, u32[]{:S(2)}) copy-start(f32[128]{0:T(128)} %param.25) | copy-start | bytes 1540
  54.3 5.0 %copy-start.2 = (bf16[256,4096]{1,0:T(8,128)(2,1)S(1)}, bf16[256,4096]{1,0:T(8,128)(2,1)}, u32[]{:S(2)}) copy-start(bf16[256,4096]{1,0:T(8,128)(2,1)} %param.26) | copy-start | bytes 6291460
  59.0 56.5 %copy-start.1 = (bf16[16,4096]{1,0:T(8,128)(2,1)S(1)}, bf16[16,4096]{1,0:T(8,128)(2,1)}, u32[]{:S(2)}) copy-start(bf16[16,4096]{1,0:T(8,128)(2,1)} %param.19) | copy-start | bytes 393220
  59.0 57.5 %copy-start.5 = (f32[4096]{0:T(1024)S(1)}, f32[4096]{0:T(1024)}, u32[]{:S(2)}) copy-start(f32[4096]{0:T(1024)} %param.30) | copy-start | bytes 49156
  60.4 100.7 %reduce-scatter.5.cloned.1.call-start = ((), (), s32[]{:S(2)}) async-start(), calls=%async_computation.7 | async-start | bytes 294912 | tf_op jit(solution)/shard_map/reduce_scatter | solution.py:112
  129.0 3.7 %copy-start.6 = (f32[16,2]{0,1:T(2,128)S(1)}, f32[16,2]{0,1:T(2,128)}, u32[]{:S(2)}) copy-start(f32[16,2]{0,1:T(2,128)} %param.34) | copy-start | bytes 388
  129.0 3.8 %copy-start.10 = (f32[16]{0:T(128)S(1)}, f32[16]{0:T(128)}, u32[]{:S(2)}) copy-start(f32[16]{0:T(128)} %param.33) | copy-start | bytes 196
  161.1 8.4 %all-to-all-start.2 = ((bf16[1,4,8,512]{3,2,0,1:T(8,128)(2,1)}), bf16[1,4,8,512]{3,2,0,1:T(8,128)(2,1)S(1)}, u32[]{:S(2)}, u32[]{:S(2)}) async-start(bf16[1,4,8,512]{3,2,0,1:T(8,128)(2,1)} %bitcast.90), calls=%async_computation.4 | async-start | bytes 65536 | tf_op jit(solution)/shard_map/all_to_all | solution.py:114
Sparse Core Ops, SparseCore 0:
  22.9 23.9 reduce-scatter.2
  60.5 54.9 all-reduce.1
  132.7 28.3 reduce-scatter.4
where the time goes:
time: 178 us
  waiting for transfers between devices  102 us (57%)
  matrix products  19.6 us (11%)
  local copies, waits for them, and re-layouts  15.5 us (9%)
  between operations  14 us (8%)
  blocking collectives  9.17 us (5%)
  starting transfers between devices  8.93 us (5%)
  other arithmetic  8.5 us (5%)
    psum x1, waiting for transfers between devices, on_device(): lax.psum(lax.optimization_barrier(term).astype(jnp.float32).astype(jnp.bf...  55 us
    reduce_scatter x1, waiting for transfers between devices, on_device(): lax.psum_scatter(down.astype(jnp.bfloat16), 'tp', scatter_dimension=2, ti...  28.4 us
    unnamed x24, local copies, waits for them, and re-layouts  13.1 us
    reduce_scatter x1, waiting for transfers between devices, on_device(): lax.psum_scatter(jnp.dot(sliced, stacked, preferred_element_type=jnp.floa...  11.5 us
    all_to_all x1, blocking collectives, on_device(): lax.all_to_all(dispatch, 'ep', split_axis=0, concat_axis=2, tiled=True)  9.17 us
    all_to_all x1, starting transfers between devices, on_device(): lax.all_to_all(normed, 'ep', split_axis=1, concat_axis=0, tiled=True)  5.19 us
    dot_general x1, matrix products, on_device(): jnp.einsum('shl,slhe->she', weights[..., :positions_all], values, preferr...  4.72 us
    all_to_all x1, waiting for transfers between devices, on_device(): lax.all_to_all(summed.reshape(experts_local, ep_count, capacity, cols), '...  4.66 us
  transfers between devices with their start and end apart: 5, of which 5 were waited for; matrix products, arithmetic and copies ran while one was open for 9% of the time, Pallas kernels for 0%

commit v1 on v0

--- a/solution.py
+++ b/solution.py
@@ -2,6 +2,7 @@
 import jax.numpy as jnp
 from jax import lax
 from jax.sharding import PartitionSpec as P
+from jax.lax import all_gather
 
 EPG = 2
 EPS = 1e-06
@@ -81,8 +82,8 @@
         .reshape(seqs, heads_local * 2 * head_dim)
     )
     term = jnp.dot(head_out, w_output, preferred_element_type=jnp.float32).astype(jnp.bfloat16)
-    attn_sum = lax.psum(
-        lax.optimization_barrier(term).astype(jnp.float32).astype(jnp.bfloat16), "tp"
+    attn_sum = jnp.sum(
+        all_gather(lax.optimization_barrier(term).astype(jnp.float32).astype(jnp.bfloat16), "tp"), 0
     ).astype(jnp.float32)
     resid = resid_in + attn_sum
     moe_in = rms_scale(resid, moe_gain).astype(jnp.bfloat16)

time: 178 us -> 146 us (0.82)
  waiting for transfers between devices: 102 us -> 70.9 us
    psum x1 -> x0, waiting for transfers between devices: 55 us -> none  [on_device(): lax.psum(lax.optimization_barrier(term).astype(jnp.float32).astype(jnp.bf...]
    all_gather x0 -> x1, waiting for transfers between devices: none -> 21.4 us  [on_device(): all_gather(lax.optimization_barrier(term).astype(jnp.float32).astype(jnp....]
    all_to_all x1, waiting for transfers between devices: 2.22 us -> 4.29 us  [on_device(): lax.all_to_all(normed, 'ep', split_axis=1, concat_axis=0, tiled=True)]
    unnamed x24 -> x28, local copies, waits for them, and re-layouts: 13.1 us -> 12.5 us
  transfers between devices with their start and end apart: 5 -> 5, of which waited for: 5 -> 5; matrix products, arithmetic and copies ran while one was open for 9% -> 10% of each run, Pallas kernels for 0% -> 0%
where the time goes in v1:
time: 146 us; the launch traced here: 145 us
  waiting for transfers between devices  70.9 us (49%)
  matrix products  18.7 us (13%)
  local copies, waits for them, and re-layouts  14.9 us (10%)
  between operations  14 us (10%)
  blocking collectives  9.56 us (7%)
  starting transfers between devices  9 us (6%)
  other arithmetic  8.32 us (6%)
    reduce_scatter x1, waiting for transfers between devices, on_device(): lax.psum_scatter(down.astype(jnp.bfloat16), 'tp', scatter_dimension=2, ti...  28.9 us
    all_gather x1, waiting for transfers between devices, on_device(): all_gather(lax.optimization_barrier(term).astype(jnp.float32).astype(jnp....  21.4 us
    unnamed x28, local copies, waits for them, and re-layouts  12.5 us
    reduce_scatter x1, waiting for transfers between devices, on_device(): lax.psum_scatter(jnp.dot(sliced, stacked, preferred_element_type=jnp.floa...  11.6 us
    all_to_all x1, blocking collectives, on_device(): lax.all_to_all(dispatch, 'ep', split_axis=0, concat_axis=2, tiled=True)  9.56 us
    all_to_all x1, starting transfers between devices, on_device(): lax.all_to_all(normed, 'ep', split_axis=1, concat_axis=0, tiled=True)  5.19 us
    dot_general x1, matrix products, on_device(): jnp.einsum('shl,slhe->she', weights[..., :positions_all], values, preferr...  4.72 us
    all_to_all x1, waiting for transfers between devices, on_device(): lax.all_to_all(summed.reshape(experts_local, ep_count, capacity, cols), '...  4.66 us
  transfers between devices with their start and end apart: 5, of which 5 were waited for; matrix products, arithmetic and copies ran while one was open for 10% of the time, Pallas kernels for 0%

profile of v1, /device:TPU:0, one launch (start us, length us, event | category | flops | bytes accessed | tf_op | source)
XLA Modules:
  0.0 145.4 jit_solution(9317695214894287143)
XLA Ops:
  7.2 1.2 fusion.27
  8.4 1.0 fusion.29
  9.4 0.6 copy.114
  10.0 5.2 %all-to-all-start = ((bf16[16,4,1024]{2,0,1:T(8,128)(2,1)}), bf16[16,4,1024]{2,0,1:T(8,128)(2,1)S(1)}, u32[]{:S(2)}, u32[]{:S(2)}) async-start(bf16[16,4,1024]{2,0,1:T(8,128)(2,1)} %bitcast.81), calls=%async_computation | async-start | bytes 262144 | tf_op jit(solution)/shard_map/all_to_all | solution.py:43
  15.2 0.7 subtract_convert_fusion
  16.0 4.3 %all-to-all-done = bf16[16,4,1024]{2,0,1:T(8,128)(2,1)S(1)} async-done(((bf16[16,4,1024]{2,0,1:T(8,128)(2,1)}), bf16[16,4,1024]{2,0,1:T(8,128)(2,1)S(1)}, u32[]{:S(2)}, u32[]{:S(2)}) %all-to-all-start) | async-done | bytes 131104 | tf_op jit(solution)/shard_map/all_to_all | solution.py:43
  20.3 2.5 %fusion.12 = f32[64,768]{1,0:T(8,128)} fusion(bf16[64,1024]{1,0:T(8,128)(2,1)S(1)} %bitcast.86, bf16[1024,256]{1,0:T(8,128)(2,1)} %param.23, bf16[1024,256]{1,0:T(8,128)(2,1)} %param.22, bf16[1024,256]{1,0:T(8,128)(2,1)} %param.21), kind=kOutput, calls=%fused_computation.16 | convolution fusion | flops 105381888 | bytes 1900544 | tf_op jit(solution)/shard_map/dot_general | solution.py:45
  22.9 12.3 %copy.78 = bf16[16,1024,256]{1,2,0:T(8,128)(2,1)} copy(bf16[16,1024,256]{2,1,0:T(8,128)(2,1)} %param.27) | data formatting | bytes 16777216 | tf_op args[8]
  35.3 11.6 %reduce-scatter.3.cloned.1.call-done = f32[16,768]{1,0:T(8,128)} async-done(((f32[64,768]{1,0:T(8,128)}), f32[16,768]{1,0:T(8,128)}) %reduce-scatter.3.cloned.1.call-update) | async-done | bytes 49168 | tf_op jit(solution)/shard_map/reduce_scatter | solution.py:44
  46.9 0.8 convert_element_type.89
  48.0 0.1 multiply_reduce_fusion.2
  48.2 4.6 %fusion.3 = f32[2,16,2,1,1024]{4,3,2,1,0:T(1,128)S(1)} fusion(bf16[16,1024,2,2,64]{1,4,3,2,0:T(8,128)(2,1)} %bitcast.82, bf16[16,2,2,64,1]{3,2,1,0,4:T(2,128)(2,1)S(1)} %reshape.202), kind=kOutput, calls=%fused_computation.4 | convolution fusion | flops 8388608 | bytes 8658944 | tf_op jit(solution)/shard_map/shcd,slhcd->cshl/dot_general | solution.py:64
  52.8 0.2 fusion.66
  53.1 0.8 fusion.35
  54.0 0.2 copy.93
  54.3 4.7 %fusion = f32[16,2,1,128]{3,2,1,0:T(1,128)S(1)} fusion(bf16[16,2,1024,1]{2,0,1,3:T(8,128)(2,1)S(1)} %slice_bitcast_fusion.2, bf16[16,1024,256]{2,1,0:T(8,128)(2,1)} %param.28), kind=kOutput, calls=%fused_computation.1 | convolution fusion | flops 8388608 | bytes 8470528 | tf_op jit(solution)/shard_map/shl,slhe->she/dot_general | solution.py:73
  59.0 0.2 multiply_reduce_fusion.3
  59.3 1.0 convolution_convert_fusion.2
  60.8 0.2 select_reduce_fusion
  61.4 21.4 %all-gather.3.cloned.1.call-done = bf16[128,4096]{1,0:T(8,128)(2,1)} async-done(((bf16[16,4096]{1,0:T(8,128)(2,1)}), bf16[128,4096]{1,0:T(8,128)(2,1)}) %all-gather.3.cloned.1.call-update) | async-done | bytes 1048592 | tf_op jit(solution)/shard_map/all_gather | solution.py:86
  82.8 1.4 reduce_sum.97
  84.2 0.2 convert_add_fusion
  84.4 0.3 fusion.5
  84.6 9.6 %all_to_all.37 = bf16[4,1,8,4096]{3,2,1,0:T(8,128)(2,1)S(1)} all-to-all(bf16[4,1,8,4096]{3,2,1,0:T(8,128)(2,1)S(1)} %fusion.5), channel_id=1, replica_groups=mesh['ep'=4,'tp'=8] {'ep'}, dimensions={0} | all-to-all | bytes 524288 | tf_op jit(solution)/shard_map/all_to_all | solution.py:107
  94.2 2.0 %fusion.10 = f32[32,256]{1,0:T(8,128)S(1)} fusion(bf16[1,4096,256]{2,1,0:T(8,128)(2,1)} %param.35, bf16[4,1,8,4096]{3,2,1,0:T(8,128)(2,1)S(1)} %all_to_all.37), kind=kOutput, calls=%fused_computation.14 | convolution fusion | flops 67108864 | bytes 2392064 | tf_op jit(solution)/shard_map/erd,edf->erf/dot_general | solution.py:109
  96.3 3.6 %fusion.6 = bf16[1,32,4096]{2,1,0:T(8,128)(2,1)} fusion(bf16[1,256,4096]{2,1,0:T(8,128)(2,1)S(1)} %copy-done, bf16[1,4096,256]{2,1,0:T(8,128)(2,1)} %param.36, bf16[4,1,8,4096]{3,2,1,0:T(8,128)(2,1)S(1)} %all_to_all.37, f32[32,256]{1,0:T(8,128)S(1)} %fusion.10), kind=kOutput, calls=%fused_computation.9 | convolution fusion | flops 134397952 | bytes 4751360 | tf_op jit(solution)/shard_map/erf,efd->erd/dot_general | solution.py:112
  100.1 28.9 %reduce-scatter.5.cloned.1.call-done = bf16[1,32,512]{2,1,0:T(8,128)(2,1)} async-done(((bf16[1,32,4096]{2,1,0:T(8,128)(2,1)}), bf16[1,32,512]{2,1,0:T(8,128)(2,1)}) %reduce-scatter.5.cloned.1.call-update) | async-done | bytes 32784 | tf_op jit(solution)/shard_map/reduce_scatter | solution.py:113
  128.9 3.7 %all-to-all-start.2 = ((bf16[1,4,8,512]{3,2,0,1:T(8,128)(2,1)}), bf16[1,4,8,512]{3,2,0,1:T(8,128)(2,1)S(1)}, u32[]{:S(2)}, u32[]{:S(2)}) async-start(bf16[1,4,8,512]{3,2,0,1:T(8,128)(2,1)} %bitcast.92), calls=%async_computation.4 | async-start | bytes 65536 | tf_op jit(solution)/shard_map/all_to_all | solution.py:115
  132.7 4.7 %all-to-all-done.2 = bf16[1,4,8,512]{3,2,0,1:T(8,128)(2,1)S(1)} async-done(((bf16[1,4,8,512]{3,2,0,1:T(8,128)(2,1)}), bf16[1,4,8,512]{3,2,0,1:T(8,128)(2,1)S(1)}, u32[]{:S(2)}, u32[]{:S(2)}) %all-to-all-start.2) | async-done | bytes 32800 | tf_op jit(solution)/shard_map/all_to_all | solution.py:115
  137.4 0.6 gather_fusion
  138.1 0.1 multiply_reduce_fusion.1
  138.2 0.6 add_convert_fusion
  (69 shorter events, 2.1 us)
Async XLA Ops:
  7.2 89.1 %copy-start = (bf16[1,256,4096]{2,1,0:T(8,128)(2,1)S(1)}, bf16[1,256,4096]{2,1,0:T(8,128)(2,1)}, u32[]{:S(2)}) copy-start(bf16[1,256,4096]{2,1,0:T(8,128)(2,1)} %param.37) | copy-start | bytes 6291460
  10.0 10.2 %all-to-all-start = ((bf16[16,4,1024]{2,0,1:T(8,128)(2,1)}), bf16[16,4,1024]{2,0,1:T(8,128)(2,1)S(1)}, u32[]{:S(2)}, u32[]{:S(2)}) async-start(bf16[16,4,1024]{2,0,1:T(8,128)(2,1)} %bitcast.81), calls=%async_computation | async-start | bytes 262144 | tf_op jit(solution)/shard_map/all_to_all | solution.py:43
  15.2 31.6 %reduce-scatter.3.cloned.1.call-start = ((), (), s32[]{:S(2)}) async-start(), calls=%async_computation.5 | async-start | bytes 245760 | tf_op jit(solution)/shard_map/reduce_scatter | solution.py:44
  20.3 2.6 %copy-start.7 = (s32[16]{0:T(128)S(1)}, s32[16]{0:T(128)}, u32[]{:S(2)}) copy-start(s32[16]{0:T(128)} %param.29) | copy-start | bytes 196
  22.8 60.0 %all-gather.3.cloned.1.call-start = ((), (), s32[]{:S(2)}) async-start(), calls=%async_computation.7 | async-start | bytes 1179648 | tf_op jit(solution)/shard_map/all_gather | solution.py:86
  47.7 5.1 %copy-start.4 = (bf16[16,256]{1,0:T(8,128)(2,1)}, bf16[16,256]{1,0:T(8,128)(2,1)S(1)}, u32[]{:S(2)}) copy-start(bf16[16,256]{1,0:T(8,128)(2,1)S(1)} %get-tuple-element.10) | copy-start | bytes 24580
  47.7 6.5 %copy-start.3 = (bf16[16,256]{1,0:T(8,128)(2,1)}, bf16[16,256]{1,0:T(8,128)(2,1)S(1)}, u32[]{:S(2)}) copy-start(bf16[16,256]{1,0:T(8,128)(2,1)S(1)} %get-tuple-element.9) | copy-start | bytes 24580
  52.8 1.1 copy-start.9
  54.2 5.0 %copy-start.10 = (f32[128]{0:T(128)S(1)}, f32[128]{0:T(128)}, u32[]{:S(2)}) copy-start(f32[128]{0:T(128)} %param.25) | copy-start | bytes 1540
  54.3 5.1 %copy-start.2 = (bf16[256,4096]{1,0:T(8,128)(2,1)S(1)}, bf16[256,4096]{1,0:T(8,128)(2,1)}, u32[]{:S(2)}) copy-start(bf16[256,4096]{1,0:T(8,128)(2,1)} %param.26) | copy-start | bytes 6291460
  59.0 1.5 %copy-start.8 = (s32[16,2]{0,1:T(2,128)S(1)}, s32[16,2]{0,1:T(2,128)}, u32[]{:S(2)}) copy-start(s32[16,2]{0,1:T(2,128)} %param.32) | copy-start | bytes 388
  59.0 1.6 %copy-start.12 = (s32[16]{0:T(128)S(1)}, s32[16]{0:T(128)}, u32[]{:S(2)}) copy-start(s32[16]{0:T(128)} %param.31) | copy-start | bytes 196
  59.0 25.2 %copy-start.1 = (bf16[16,4096]{1,0:T(8,128)(2,1)S(1)}, bf16[16,4096]{1,0:T(8,128)(2,1)}, u32[]{:S(2)}) copy-start(bf16[16,4096]{1,0:T(8,128)(2,1)} %param.19) | copy-start | bytes 393220
  59.3 25.0 %copy-start.5 = (f32[4096]{0:T(1024)S(1)}, f32[4096]{0:T(1024)}, u32[]{:S(2)}) copy-start(f32[4096]{0:T(1024)} %param.30) | copy-start | bytes 49156
  60.4 68.5 %reduce-scatter.5.cloned.1.call-start = ((), (), s32[]{:S(2)}) async-start(), calls=%async_computation.6 | async-start | bytes 294912 | tf_op jit(solution)/shard_map/reduce_scatter | solution.py:113
  96.3 3.7 %copy-start.6 = (f32[16,2]{0,1:T(2,128)S(1)}, f32[16,2]{0,1:T(2,128)}, u32[]{:S(2)}) copy-start(f32[16,2]{0,1:T(2,128)} %param.34) | copy-start | bytes 388
  96.3 3.8 %copy-start.11 = (f32[16]{0:T(128)S(1)}, f32[16]{0:T(128)}, u32[]{:S(2)}) copy-start(f32[16]{0:T(128)} %param.33) | copy-start | bytes 196
  128.9 8.5 %all-to-all-start.2 = ((bf16[1,4,8,512]{3,2,0,1:T(8,128)(2,1)}), bf16[1,4,8,512]{3,2,0,1:T(8,128)(2,1)S(1)}, u32[]{:S(2)}, u32[]{:S(2)}) async-start(bf16[1,4,8,512]{3,2,0,1:T(8,128)(2,1)} %bitcast.92), calls=%async_computation.4 | async-start | bytes 65536 | tf_op jit(solution)/shard_map/all_to_all | solution.py:115
Sparse Core Ops, SparseCore 0:
  22.9 23.9 reduce-scatter.2
  60.5 22.2 all-gather.2
  100.0 28.8 reduce-scatter.4
